TPU v7x, 32 devices: a whole 2x2x4 slice. The times are simulated.
32 devices in a mesh: sp: 8 (over z, x), tp: 4 (over y, core).
Axes of the slice: x: 2, y: 2, z: 4, core: 2. Of those that a mesh axis runs over, the one named last changes fastest.
Arguments:
- tokens: bfloat16 [1536, 2048], P(('sp', 'tp')), may hold values from -7 to 7
- input_norm_gain: float32 [2048], replicated, may hold values from 0.1 to 1.9
- paired_query_weight: bfloat16 [2048, 512], P('sp', 'tp'), may hold values from -16 to 16
- shared_key_weight: bfloat16 [2048, 64], replicated, may hold values from -1 to 1
- shared_value_weight: bfloat16 [2048, 64], replicated, may hold values from -0.125 to 0.125
- recurrent_query_weight: bfloat16 [2048, 1024], P('sp', 'tp'), may hold values from -0.125 to 0.125
- forget_gate_weight: bfloat16 [2048, 1024], P('sp', 'tp'), may hold values from -0.125 to 0.125
- recurrent_value_weight: bfloat16 [2048, 1024], P('sp', 'tp'), may hold values from -0.125 to 0.125
- attention_output_weight: bfloat16 [2048, 512], P('sp', 'tp'), may hold values from -0.15625 to 0.15625
- recurrent_output_weight: bfloat16 [2048, 1024], P('sp', 'tp'), may hold values from -0.15625 to 0.15625
- attention_head_gain: float32 [64], replicated, may hold values from 0.1 to 1.9
- recurrent_head_gain: float32 [128], replicated, may hold values from 0.1 to 1.9
- second_map_weight: float32 [8], P('tp'), may hold values from 0.3 to 0.8
- forget_leak_rate: float32 [1024], P('tp'), may hold values from 2e-05 to 0.05
- extra_log_decay: float32 [1536, 1024], P('sp', 'tp'), may hold values from -1 to 0
- initial_recurrent_state: float32 [8, 128, 128], P('tp'), may hold values from -0.12 to 0.12
Outputs:
- mixer_out: bfloat16 [1536, 2048], P(('sp', 'tp'))
All inputs are finite; a program needn't handle non-finite values.
Results may differ from a plain program's by a relative error of at most 0.014.
Values may be sent and summed in bfloat16 or wider, within the bound.
A program may use at most 128 MiB of HBM per device.

v0:
```python
import math

import jax
import jax.numpy as jnp
from jax import lax
from jax.sharding import PartitionSpec as P

QK_DIM = 32
HEAD_DIM = 64
RECURRENT_WIDTH = 128
REC_SPAN = 64


epsilon = 1e-06
highest_precision = lax.Precision.HIGHEST


def entering(x, axis, combine, identity):
    size, mine = (lax.axis_size(axis), lax.axis_index(axis))
    everything = jax.tree.map(
        lambda part, kind: lax.all_gather(part.astype(kind), axis), x, (jnp.bfloat16, jnp.bfloat16)
    )
    start = jax.tree.map(
        lambda part, zero: jnp.broadcast_to(jnp.asarray(zero, part.dtype), part.shape), x, identity
    )

    def entering_turn(k, before):
        reached = k < mine
        new = combine(
            before, jax.tree.map(lambda part, own: part[k].astype(own.dtype), everything, x)
        )
        return jax.tree.map(lambda a, b: jnp.where(reached, a, b), new, before)

    return lax.fori_loop(0, size, entering_turn, start)


def rms_scale(matrix, gain):
    return matrix * lax.rsqrt(jnp.mean(matrix * matrix, axis=-1, keepdims=True) + epsilon) * gain


def project(normed, weight):
    return jnp.dot(normed, weight, preferred_element_type=jnp.float32).astype(jnp.bfloat16)


def widen(stored):
    return lax.optimization_barrier(stored).astype(jnp.float32)


def absorb(partial_state, queries, key_block, value_block):
    peak_score, totals, weighted = partial_state
    key_split = key_block.reshape(key_block.shape[0], 2, QK_DIM)
    scores = jnp.einsum(
        "thcd,jcd->chtj", queries, key_split, preferred_element_type=jnp.float32
    ) * (1.0 / math.sqrt(QK_DIM))
    new_peak = jnp.maximum(peak_score, jnp.max(scores, axis=3))
    shrink = jnp.exp(peak_score - new_peak)
    expo_terms = jnp.exp(scores - new_peak[..., None])
    totals = totals * shrink + jnp.sum(expo_terms, axis=3)
    weighted = weighted * shrink[..., None] + jnp.einsum(
        "chtj,jv->chtv",
        expo_terms.astype(jnp.bfloat16),
        value_block,
        preferred_element_type=jnp.float32,
    )
    return (new_peak, totals, weighted)


def fold_keys(queries):

    def visit_piece(partial_state, piece, start_row):
        keys_piece, values_piece = piece
        piece_rows = keys_piece.shape[0]
        block_rows = min(piece_rows, 512)
        full_count = piece_rows // block_rows

        def visit_turn(turn_index, running_state):
            begin_row = turn_index * block_rows
            return absorb(
                running_state,
                queries,
                lax.dynamic_slice_in_dim(keys_piece, begin_row, block_rows, 0),
                lax.dynamic_slice_in_dim(values_piece, begin_row, block_rows, 0),
            )

        partial_state = lax.fori_loop(0, full_count, visit_turn, partial_state)
        return partial_state

    return visit_piece


def span_scan(rec_query, inflow_state, rec_values, log_decay_values):
    head_count, row_count, channel_width = rec_query.shape
    span_count = row_count // REC_SPAN

    def to_spans(matrix):
        return jnp.moveaxis(
            matrix.reshape(head_count, span_count, REC_SPAN, matrix.shape[-1]), 1, 0
        )

    lower_mask = jnp.tril(jnp.ones((REC_SPAN, REC_SPAN), jnp.float32))

    def step(carry_pair, inputs):
        carried_state, offset = carry_pair
        query_span, inflow_span, value_segment, decay_span = inputs
        running = jnp.cumsum(decay_span, axis=1)
        segment_final = running[:, -1:, :]
        decayed_query = query_span * jnp.exp(running)
        inflow_dec = inflow_span * jnp.exp(-running)
        within_segment = (
            jnp.einsum("hsk,htk->hst", decayed_query, inflow_dec, precision=highest_precision)
            * lower_mask
        )
        segment_output = jnp.einsum(
            "rcn,rni->rci", within_segment, value_segment, precision=highest_precision
        ) + jnp.einsum("cwi,cip->cwp", decayed_query, carried_state, precision=highest_precision)
        lifted_values = query_span * jnp.exp(offset + running)
        inflow_final = inflow_span * jnp.exp(segment_final - running)
        carried_state = jnp.exp(segment_final)[:, 0, :, None] * carried_state + jnp.einsum(
            "rgc,rgt->rct", inflow_final, value_segment, precision=highest_precision
        )
        return ((carried_state, offset + segment_final), (segment_output, lifted_values))

    initial = (
        jnp.zeros((head_count, channel_width, rec_values.shape[-1]), jnp.float32),
        jnp.zeros((head_count, 1, channel_width), jnp.float32),
    )
    (final_state, offset), (span_outs, lifted_all) = lax.scan(
        step,
        initial,
        (
            to_spans(rec_query),
            to_spans(inflow_state),
            to_spans(rec_values),
            to_spans(log_decay_values),
        ),
    )
    local_output = jnp.moveaxis(span_outs, 0, 1).reshape(
        head_count, row_count, rec_values.shape[-1]
    )
    lifted_values = jnp.moveaxis(lifted_all, 0, 1).reshape(head_count, row_count, channel_width)
    return (final_state, local_output, lifted_values, jnp.exp(offset[:, 0, :]))


def body(
    tokens,
    input_norm_gain,
    paired_query_weight,
    shared_key_weight,
    shared_value_weight,
    recurrent_query_weight,
    forget_gate_weight,
    recurrent_value_weight,
    attention_output_weight,
    recurrent_output_weight,
    attention_head_gain,
    recurrent_head_gain,
    second_map_weight,
    forget_leak_rate,
    extra_log_decay,
    initial_recurrent_state,
):
    own_normed = rms_scale(tokens.astype(jnp.float32), input_norm_gain).astype(jnp.bfloat16)
    normed = lax.all_gather(own_normed, "tp", axis=0, tiled=True)
    row_count = normed.shape[0]
    weights = (
        lax.all_gather(paired_query_weight, "sp", axis=0, tiled=True),
        lax.all_gather(recurrent_query_weight, "sp", axis=0, tiled=True),
        lax.all_gather(forget_gate_weight, "sp", axis=0, tiled=True),
        lax.all_gather(recurrent_value_weight, "sp", axis=0, tiled=True),
        lax.all_gather(attention_output_weight, "sp", axis=0, tiled=True),
        lax.all_gather(recurrent_output_weight, "sp", axis=0, tiled=True),
    )
    attn_heads = paired_query_weight.shape[1] // (2 * QK_DIM)
    rec_heads = recurrent_query_weight.shape[1] // RECURRENT_WIDTH
    queries = project(normed, weights[0]).reshape(row_count, attn_heads, 2, QK_DIM)
    initial = (
        jnp.full((2, attn_heads, row_count), -jnp.inf, jnp.float32),
        jnp.zeros((2, attn_heads, row_count), jnp.float32),
        jnp.zeros((2, attn_heads, row_count, HEAD_DIM), jnp.float32),
    )
    visit_piece = fold_keys(queries)
    peak_score, totals, weighted = visit_piece(
        initial,
        (
            lax.all_gather(project(normed, shared_key_weight), "sp", axis=0, tiled=True),
            lax.all_gather(project(normed, shared_value_weight), "sp", axis=0, tiled=True),
        ),
        jnp.int32(0),
    )
    primary = weighted[0] / totals[0][..., None]
    secondary = weighted[1] / totals[1][..., None]
    blended = primary - second_map_weight[:, None, None] * secondary
    attn_hidden = (
        rms_scale(blended, attention_head_gain)
        .transpose(1, 0, 2)
        .reshape(row_count, attn_heads * HEAD_DIM)
        .astype(jnp.bfloat16)
    )
    rec_query = jax.nn.silu(widen(project(normed, weights[1])))
    gate_raw = widen(project(normed, weights[2]))
    rec_values = widen(project(normed, weights[3]))
    inflow_state = forget_leak_rate * (1.0 - jax.nn.sigmoid(gate_raw))
    log_decay_values = jnp.log(1.0 - inflow_state) + extra_log_decay

    def heads_first(matrix):
        return matrix.reshape(row_count, rec_heads, RECURRENT_WIDTH).transpose(1, 0, 2)

    local_state, local_output, lifted_values, reach_decay = span_scan(
        heads_first(rec_query),
        heads_first(inflow_state),
        heads_first(rec_values),
        heads_first(log_decay_values),
    )

    def chain_step(earlier, later):
        return (earlier[0] * later[0], later[0][..., None] * earlier[1] + later[1])

    identity = (jnp.ones_like(reach_decay), jnp.zeros_like(local_state))
    prior_decay, prior_state = entering((reach_decay, local_state), "sp", chain_step, identity)
    incoming_state = prior_decay[..., None] * initial_recurrent_state + prior_state
    recurrent_output = local_output + jnp.einsum(
        "cwi,cip->cwp", lifted_values, incoming_state, precision=highest_precision
    )
    rec_hidden = (
        rms_scale(recurrent_output, recurrent_head_gain)
        .transpose(1, 0, 2)
        .reshape(row_count, rec_heads * RECURRENT_WIDTH)
        .astype(jnp.bfloat16)
    )
    return lax.psum_scatter(
        (
            jnp.einsum("tk,dk->td", attn_hidden, weights[4], preferred_element_type=jnp.float32)
            + jnp.einsum("tk,dk->td", rec_hidden, weights[5], preferred_element_type=jnp.float32)
        ).astype(jnp.bfloat16),
        "tp",
        scatter_dimension=0,
        tiled=True,
    )


def solution(mesh):
    placed = (
        P(("sp", "tp"), None),
        P(),
        P("sp", "tp"),
        P(),
        P(),
        P("sp", "tp"),
        P("sp", "tp"),
        P("sp", "tp"),
        P("sp", "tp"),
        P("sp", "tp"),
        P(),
        P(),
        P("tp"),
        P("tp"),
        P("sp", "tp"),
        P("tp", None, None),
    )
    return jax.shard_map(
        body, mesh=mesh, in_specs=placed, out_specs=P(("sp", "tp"), None), check_vma=False
    )
```

profile of v0, /device:TPU:0, one launch (start us, length us, event | category | flops | bytes accessed | tf_op | source)
XLA Modules:
  0.0 254.0 jit_solution(1802197610598582858)
XLA Ops:
  6.5 0.7 all-gather.9.cloned.1.call-update
  7.3 0.7 all-gather.11.cloned.1.call-update
  8.1 0.7 all-gather.13.cloned.1.call-update
  8.8 0.5 all-gather.15.cloned.1.call-update
  9.5 1.1 fusion.40
  10.5 1.1 fusion.42
  11.6 10.2 %all_gather.37 = bf16[192,2048]{1,0:T(8,128)(2,1)S(1)} all-gather(bf16[48,2048]{1,0:T(8,128)(2,1)S(1)} %fusion.42), channel_id=1, replica_groups=mesh['sp'=8,'tp'=4] {'tp'}, dimensions={0}, use_global_device_ids=true | all-gather | bytes 983040 | tf_op jit(solution)/shard_map/all_gather | solution.py:163
  21.8 0.4 fusion.38
  22.2 31.6 %all-gather.2 = bf16[8,192,64]{1,2,0:T(8,128)(2,1)S(1)} all-gather(bf16[1,192,64]{1,2,0:T(8,128)(2,1)S(1)} %fusion.38), channel_id=1, replica_groups=mesh['sp'=8,'tp'=4] {'sp'}, dimensions={0}, use_global_device_ids=true | all-gather | bytes 221184 | tf_op jit(solution)/shard_map/all_gather | solution.py:185
  54.0 0.9 reshape.136
  54.9 0.4 fusion.39
  55.3 31.4 %all-gather.3 = bf16[8,192,64]{1,2,0:T(8,128)(2,1)S(1)} all-gather(bf16[1,192,64]{1,2,0:T(8,128)(2,1)S(1)} %fusion.39), channel_id=1, replica_groups=mesh['sp'=8,'tp'=4] {'sp'}, dimensions={0}, use_global_device_ids=true | all-gather | bytes 221184 | tf_op jit(solution)/shard_map/all_gather | solution.py:186
  87.1 31.7 %all_gather.39 = bf16[2048,128]{1,0:T(8,128)(2,1)S(1)} all-gather(bf16[256,128]{1,0:T(8,128)(2,1)S(1)} %copy-done.7), channel_id=1, replica_groups=mesh['sp'=8,'tp'=4] {'sp'}, dimensions={0}, use_global_device_ids=true | all-gather | bytes 589824 | tf_op jit(solution)/shard_map/all_gather | solution.py:166
  118.8 0.4 convolution_convert_fusion.3
  119.3 7.5 %while.51 = (s32[]{:T(128)}, f32[2,2,192]{2,1,0:T(2,128)S(1)}, f32[2,2,192]{2,1,0:T(2,128)S(1)}, f32[2,2,192,64]{2,3,1,0:T(8,128)S(1)}, bf16[1536,64]{0,1:T(8,12...) while((s32[]{:T(128)}, f32[2,2,192]{2,1,0:T(2,128)S(1)}, ...), condition=%wide.region_4.0_spmd.clone, body=%wide.region_1.0_spmd.clone.sunk | while | flops 78008064 | bytes 5540015 | solution.py:85
  119.3 0.9 constant_dynamic-slice_fusion.2
  120.2 0.5 bitcast_reduce_fusion.2
  120.7 0.5 fusion.100
  121.3 0.5 convolution_add_fusion.7
  121.8 0.8 constant_dynamic-slice_fusion.2
  122.7 0.5 bitcast_reduce_fusion.2
  123.2 0.5 fusion.100
  123.8 0.5 convolution_add_fusion.7
  124.3 0.8 constant_dynamic-slice_fusion.2
  125.2 0.5 bitcast_reduce_fusion.2
  125.7 0.5 fusion.100
  126.3 0.5 convolution_add_fusion.7
  127.0 32.2 %all_gather.41 = bf16[2048,128]{1,0:T(8,128)(2,1)S(1)} all-gather(bf16[256,128]{1,0:T(8,128)(2,1)S(1)} %copy-done.8), channel_id=1, replica_groups=mesh['sp'=8,'tp'=4] {'sp'}, dimensions={0}, use_global_device_ids=true | all-gather | bytes 589824 | tf_op jit(solution)/shard_map/all_gather | solution.py:170
  159.3 1.6 fusion.57
  160.9 1.6 convolution_convert_fusion.2
  162.5 1.6 convolution_convert_fusion.1
  164.2 1.7 convolution_convert_fusion
  166.2 4.0 %while.52 = (s32[]{:T(128)}, f32[2,128,128]{2,1,0:T(8,128)S(1)}, f32[2,1,128]{2,1,0:T(1,128)S(1)}, f32[3,2,64,128]{3,2,1,0:T(8,128)S(1)}, f32[3,2,64,128]{3,2,0,...) while((s32[]{:T(128)}, f32[2,128,128]{2,1,0:T(8,128)S(1)}, ...), condition=%wide.region_8.9_spmd.clone, body=%wide.region_6.8_spmd.clone.sunk | while | flops 76825088 | bytes 1863825 | solution.py:127
  166.4 0.2 convolution_multiply_fusion.3
  166.8 0.3 fusion.108
  167.1 0.4 convolution_add_fusion.8
  167.7 0.2 convolution_multiply_fusion.3
  168.2 0.3 fusion.108
  168.4 0.4 convolution_add_fusion.8
  169.0 0.2 convolution_multiply_fusion.3
  169.5 0.3 fusion.108
  169.8 0.4 convolution_add_fusion.8
  170.3 31.8 %all-gather.1 = bf16[16,128,128]{2,1,0:T(8,128)(2,1)S(1)} all-gather(bf16[2,128,128]{2,1,0:T(8,128)(2,1)S(1)} %convert_element_type.116), channel_id=3, replica_groups=mesh['sp'=8,'tp'=4] {'sp'}, dimensions={0}, use_global_device_ids=true | all-gather | bytes 589824 | tf_op jit(solution)/shard_map/all_gather | solution.py:21
  202.0 20.1 %all-gather = bf16[16,1,128]{2,1,0:T(2,128)(2,1)S(1)} all-gather(bf16[2,1,128]{2,1,0:T(2,128)(2,1)S(1)} %exponential_convert_fusion), channel_id=2, replica_groups=mesh['sp'=8,'tp'=4] {'sp'}, dimensions={0}, use_global_device_ids=true | all-gather | bytes 4608 | tf_op jit(solution)/shard_map/all_gather | solution.py:21
  222.2 1.5 while.53
  223.7 0.5 multiply_reduce_fusion
  224.3 2.6 %fusion.37 = bf16[192,2048]{1,0:T(8,128)(2,1)} fusion(f32[192,2048]{1,0:T(8,128)S(1)} %copy-done.1, bf16[2048,256]{1,0:T(8,128)(2,1)} %all-gather.15.cloned.1.call-done, f32[2,192,128]{2,1,0:T(8,128)S(1)} %get-tuple-element.478, f32[128]{0:T(128)S(1)} %copy-done.12, f32[2,192]{1,0:T(2,128)S(1)} %add_rsqrt_fusion), kind=kOutput, calls=%fused_computation.62 | convolution fusion | flops 202260480 | bytes 3606528 | tf_op jit(solution)/shard_map/tk,dk->td/dot_general | solution.py:233
  227.0 20.5 %reduce-scatter.2.cloned.1.call-done = bf16[48,2048]{1,0:T(8,128)(2,1)} async-done(((bf16[192,2048]{1,0:T(8,128)(2,1)}), bf16[48,2048]{1,0:T(8,128)(2,1)}) %reduce-scatter.2.cloned.1.call-update) | async-done | bytes 196624 | tf_op jit(solution)/shard_map/reduce_scatter | solution.py:230
  (115 shorter events, 3.8 us)
Async XLA Ops:
  6.5 15.3 %copy-start = (bf16[2048,64]{0,1:T(8,128)(2,1)S(1)}, bf16[2048,64]{0,1:T(8,128)(2,1)}, u32[]{:S(2)}) copy-start(bf16[2048,64]{0,1:T(8,128)(2,1)} %param.25) | copy-start | bytes 786436
  6.5 154.3 %all-gather.9.cloned.1.call-start = ((), (), s32[]{:S(2)}) async-start(), calls=%async_computation.1 | async-start | bytes 1179648 | tf_op jit(solution)/shard_map/all_gather | solution.py:168
  7.3 155.2 %all-gather.11.cloned.1.call-start = ((), (), s32[]{:S(2)}) async-start(), calls=%async_computation.2 | async-start | bytes 1179648 | tf_op jit(solution)/shard_map/all_gather | solution.py:169
  8.0 156.2 %all-gather.13.cloned.1.call-start = ((), (), s32[]{:S(2)}) async-start(), calls=%async_computation.3 | async-start | bytes 1179648 | tf_op jit(solution)/shard_map/all_gather | solution.py:167
  8.7 215.6 %all-gather.15.cloned.1.call-start = ((), (), s32[]{:S(2)}) async-start(), calls=%async_computation.4 | async-start | bytes 1179648 | tf_op jit(solution)/shard_map/all_gather | solution.py:171
  9.3 238.2 %reduce-scatter.2.cloned.1.call-start = ((), (), s32[]{:S(2)}) async-start(), calls=%async_computation.5 | async-start | bytes 983040 | tf_op jit(solution)/shard_map/reduce_scatter | solution.py:230
  11.6 43.3 %copy-start.2 = (bf16[2048,64]{0,1:T(8,128)(2,1)S(1)}, bf16[2048,64]{0,1:T(8,128)(2,1)}, u32[]{:S(2)}) copy-start(bf16[2048,64]{0,1:T(8,128)(2,1)} %param.26) | copy-start | bytes 786436
  53.8 33.2 %copy-start.7 = (bf16[256,128]{1,0:T(8,128)(2,1)S(1)}, bf16[256,128]{1,0:T(8,128)(2,1)}, u32[]{:S(2)}) copy-start(bf16[256,128]{1,0:T(8,128)(2,1)} %param.24) | copy-start | bytes 196612
  119.3 7.6 %copy-start.10 = (f32[2]{0:T(128)S(1)}, f32[2]{0:T(128)}, u32[]{:S(2)}) copy-start(f32[2]{0:T(128)} %param.34) | copy-start | bytes 28
  119.3 7.7 %copy-start.8 = (bf16[256,128]{1,0:T(8,128)(2,1)S(1)}, bf16[256,128]{1,0:T(8,128)(2,1)}, u32[]{:S(2)}) copy-start(bf16[256,128]{1,0:T(8,128)(2,1)} %param.30) | copy-start | bytes 196612
  119.3 39.9 %copy-start.11 = (f32[64]{0:T(128)S(1)}, f32[64]{0:T(128)}, u32[]{:S(2)}) copy-start(f32[64]{0:T(128)} %param.32) | copy-start | bytes 772
  164.1 1.9 copy-start.4
  164.1 1.9 copy-start.9
  164.2 2.0 copy-start.3
  164.2 2.0 copy-start.5
  170.2 53.5 %copy-start.6 = (f32[2,128,128]{2,1,0:T(8,128)S(1)}, f32[2,128,128]{2,1,0:T(8,128)}, u32[]{:S(2)}) copy-start(f32[2,128,128]{2,1,0:T(8,128)} %param.37) | copy-start | bytes 393220
  202.0 22.3 %copy-start.1 = (f32[192,2048]{1,0:T(8,128)S(1)}, f32[192,2048]{1,0:T(8,128)}, u32[]{:S(2)}) copy-start(f32[192,2048]{1,0:T(8,128)} %fusion.57) | copy-start | bytes 4718596
  202.0 22.3 %copy-start.12 = (f32[128]{0:T(128)S(1)}, f32[128]{0:T(128)}, u32[]{:S(2)}) copy-start(f32[128]{0:T(128)} %param.33) | copy-start | bytes 1540
Sparse Core Ops, SparseCore 0:
  9.5 44.5 all-gather.8
  56.1 40.1 all-gather.10
  98.5 42.0 all-gather.12
  142.6 41.8 all-gather.14
  227.1 20.3 reduce-scatter.1
where the time goes:
time: 255 us; the launch traced here: 254 us
  blocking collectives  189 us (74%)
  waiting for transfers between devices  23.2 us (9%)
  matrix products  17.3 us (7%)
  between operations  13.5 us (5%)
  other arithmetic  5.89 us (2%)
  local copies, waits for them, and re-layouts  4.28 us (2%)
    all_gather x2, blocking collectives, entering(): lax.all_gather(part.astype(kind), axis)  51.9 us
    all_gather x1, blocking collectives, body(): lax.all_gather(attention_output_weight, 'sp', axis=0, tiled=True)  32.2 us
    all_gather x1, blocking collectives, body(): lax.all_gather(paired_query_weight, 'sp', axis=0, tiled=True)  31.7 us
    all_gather x1, blocking collectives, body(): lax.all_gather(project(normed, shared_key_weight), 'sp', axis=0, tiled=True)  31.6 us
    all_gather x1, blocking collectives, body(): lax.all_gather(project(normed, shared_value_weight), 'sp', axis=0, tiled=...  31.4 us
    reduce_scatter x1, waiting for transfers between devices, body(): lax.psum_scatter((jnp.einsum('tk,dk->td', attn_hidden, weights[4], prefer...  20.5 us
    all_gather x1, blocking collectives, body(): normed = lax.all_gather(own_normed, 'tp', axis=0, tiled=True)  10.2 us
    dot_general x6, matrix products, project(): jnp.dot(normed, weight, preferred_element_type=jnp.float32)  6.05 us
  transfers between devices with their start and end apart: 5, of which 1 were waited for; matrix products, arithmetic and copies ran while one was open for 10% of the time, Pallas kernels for 0%

commit v1 on v0

v1 whole, which is shorter than its diff:
```python
import functools
import math

import jax
import jax.numpy as jnp
from jax import lax
from jax.experimental import pallas as pl
from jax.experimental.pallas import tpu as pltpu
from jax.sharding import PartitionSpec as P

QK_DIM = 32
HEAD_DIM = 64
RECURRENT_WIDTH = 128
REC_SPAN = 64
KEY_BLOCK = 1536
EPS = 1e-06
MESH = pl.DeviceIdType.MESH
F32, BF16 = jnp.float32, jnp.bfloat16

NN = (((1,), (0,)), ((), ()))
NT = (((1,), (1,)), ((), ()))
TN = (((0,), (0,)), ((), ()))


def dot(a, b, dims=NN, precision=None):
    return lax.dot_general(a, b, dims, preferred_element_type=F32, precision=precision)


def rms(x, gain):
    return x * lax.rsqrt(jnp.mean(x * x, axis=-1, keepdims=True) + EPS) * gain


def loop(lo, hi, body):
    def step(j, carry):
        body(j)
        return carry

    lax.fori_loop(lo, hi, step, 0)


def kernel(
    n, nt,
    tok, gain, wq, wg, wv, wr, woa, wor, wk, wval, again, rgain, mapw, leak, extra, init,
    out,
    gq, gg, gv, gr, goa, gor, nf, kv, state, decay, pbuf, rbuf,
    ring_send, ring_recv, n_send, n_recv, kv_send, kv_recv, kt_send, kt_recv,
    st_send, st_recv, de_send, de_recv, o_send, o_recv,
):
    s, t = lax.axis_index("sp"), lax.axis_index("tp")
    half = n // 2
    x, z = s % 2, s // 2
    pos = (1 - x) * z + x * (n - 1 - z)

    def at(p):
        p = (p + 2 * n) % n
        hi = p // half
        return (1 - hi) * 2 * p + hi * (2 * (n - 1 - p) + 1)

    ins = (wq, wg, wv, wr, woa, wor)
    bufs = (gq, gg, gv, gr, goa, gor)
    longer = (0, 0, 1, 0, 1, 1)

    def hops(a, d):
        return half if longer[a] == d else half - 1

    def send(a, d, k, first):
        sign = 1 - 2 * d
        owner = s if first else at(pos - sign * k)
        return pltpu.make_async_remote_copy(
            src_ref=ins[a] if first else bufs[a].at[owner],
            dst_ref=bufs[a].at[owner],
            send_sem=ring_send.at[a, d, k],
            recv_sem=ring_recv.at[a, d, k],
            device_id=(at(pos + sign), t),
            device_id_type=MESH,
        )

    def arrival(a, d, k):
        sign = 1 - 2 * d
        slot = bufs[a].at[at(pos - sign * (k + 1))]
        return pltpu.make_async_remote_copy(
            src_ref=slot, dst_ref=slot,
            send_sem=ring_send.at[a, d, k], recv_sem=ring_recv.at[a, d, k],
            device_id=(at(pos - sign), t), device_id_type=MESH,
        )

    def start(group):
        for a in group:
            for d in (0, 1):
                send(a, d, 0, True).start()

    def ring_hop(group, k):
        for a in group:
            for d in (0, 1):
                count = hops(a, d)

                @pl.when(k < count)
                def _():
                    arrival(a, d, k).wait_recv()

                @pl.when(k + 1 < count)
                def _():
                    send(a, d, k + 1, False).start()

    def ring(group, lo, hi):
        if n <= 8:
            for k in range(lo, hi):
                ring_hop(group, k)
        else:
            loop(lo, hi, lambda k: ring_hop(group, k))

    def finish(group):
        for a in group:
            for d in (0, 1):
                send(a, d, 0, True).wait_send()
                loop(1, hops(a, d), lambda k: send(a, d, k, False).wait_send())

    one, two = (0, 1, 2), (3, 4, 5)
    cut = [half * i // 4 for i in range(5)]
    start(one)

    rows = tok.shape[0]
    normed = rms(tok[...].astype(F32), gain[...]).astype(BF16)
    nf[t] = normed

    def tp_peer(j):
        return (t + j) % nt

    def n_copy(j):
        return pltpu.make_async_remote_copy(
            src_ref=nf.at[t], dst_ref=nf.at[t], send_sem=n_send.at[j], recv_sem=n_recv.at[j],
            device_id=(s, tp_peer(j)), device_id_type=MESH,
        )

    def n_in(j):
        slot = nf.at[(t + nt - j) % nt]
        return pltpu.make_async_remote_copy(
            src_ref=slot, dst_ref=slot, send_sem=n_send.at[j], recv_sem=n_recv.at[j],
            device_id=(s, (t + nt - j) % nt), device_id_type=MESH,
        )

    kv[t, s] = jnp.concatenate(
        [dot(normed, wk[...]).astype(BF16), dot(normed, wval[...]).astype(BF16)], axis=1
    )
    for j in range(1, nt):
        n_copy(j).start()

    def kv_copy(j):
        return pltpu.make_async_remote_copy(
            src_ref=kv.at[t, s], dst_ref=kv.at[t, s],
            send_sem=kv_send.at[j], recv_sem=kv_recv.at[j],
            device_id=((s + j) % n, t), device_id_type=MESH,
        )

    def kv_in(j):
        slot = kv.at[t, (s + n - j) % n]
        return pltpu.make_async_remote_copy(
            src_ref=slot, dst_ref=slot, send_sem=kv_send.at[j], recv_sem=kv_recv.at[j],
            device_id=((s + n - j) % n, t), device_id_type=MESH,
        )

    def kt_copy(j):
        return pltpu.make_async_remote_copy(
            src_ref=kv.at[t], dst_ref=kv.at[t], send_sem=kt_send.at[j], recv_sem=kt_recv.at[j],
            device_id=(s, tp_peer(j)), device_id_type=MESH,
        )

    def kt_in(j):
        slot = kv.at[(t + nt - j) % nt]
        return pltpu.make_async_remote_copy(
            src_ref=slot, dst_ref=slot, send_sem=kt_send.at[j], recv_sem=kt_recv.at[j],
            device_id=(s, (t + nt - j) % nt), device_id_type=MESH,
        )

    loop(1, n, lambda j: kv_copy(j).start())
    for a in range(6):
        bufs[a][s] = ins[a][...]

    ring(one, 0, max(cut[1], 1))
    loop(1, n, lambda j: kv_in(j).wait_recv())
    for j in range(1, nt):
        kt_copy(j).start()
    ring(one, max(cut[1], 1), half - 1)
    start(two)
    for j in range(1, nt):
        n_in(j).wait_recv()
        kt_in(j).wait_recv()
    ring(one, half - 1, half)

    count = nt * rows
    full = nf[...].reshape(count, nf.shape[2])

    def project(buf):
        return dot(full, buf[...].reshape(full.shape[1], buf.shape[2])).astype(BF16)

    queries = project(gq)
    gate = project(gg).astype(F32)
    vals = project(gv)
    ring(two, cut[0], cut[1])

    inflow = leak[...] * (1.0 - jax.nn.sigmoid(gate))
    log_decay = jnp.log(1.0 - inflow) + extra[...]
    spans = count // REC_SPAN
    rr = lax.broadcasted_iota(jnp.int32, (REC_SPAN, REC_SPAN), 0)
    cc = lax.broadcasted_iota(jnp.int32, (REC_SPAN, REC_SPAN), 1)
    lower = (rr >= cc).astype(F32)
    running, offsets = [], []
    offset = jnp.zeros((1, log_decay.shape[1]), F32)
    for i in range(spans):
        part = log_decay[i * REC_SPAN : (i + 1) * REC_SPAN]
        run = dot(lower, part, precision=lax.Precision.HIGHEST)
        running.append(run)
        offsets.append(offset)
        offset = offset + run[REC_SPAN - 1 : REC_SPAN]
    total = offset
    heads = log_decay.shape[1] // RECURRENT_WIDTH
    befores = [[None] * spans for _ in range(heads)]
    for h in range(heads):
        c = slice(h * RECURRENT_WIDTH, (h + 1) * RECURRENT_WIDTH)
        carried = None
        for i in range(spans):
            r = slice(i * REC_SPAN, (i + 1) * REC_SPAN)
            befores[h][i] = carried
            final = running[i][REC_SPAN - 1 : REC_SPAN, c]
            weight = (inflow[r, c] * jnp.exp(final - running[i][:, c])).astype(BF16)
            new = dot(vals[r, c], weight, TN)
            carried = new if carried is None else carried * jnp.exp(final) + new
        state[s, h] = carried.astype(BF16)
    decay[s] = jnp.broadcast_to(total, decay.shape[1:])

    def st_pair(j, peer, owner):
        return (
            pltpu.make_async_remote_copy(
                src_ref=state.at[owner], dst_ref=state.at[owner],
                send_sem=st_send.at[j], recv_sem=st_recv.at[j],
                device_id=(peer, t), device_id_type=MESH,
            ),
            pltpu.make_async_remote_copy(
                src_ref=decay.at[owner], dst_ref=decay.at[owner],
                send_sem=de_send.at[j], recv_sem=de_recv.at[j],
                device_id=(peer, t), device_id_type=MESH,
            ),
        )

    def st_start(j):
        for copy in st_pair(j, s + j, s):
            copy.start()

    def st_wait(j):
        for copy in st_pair(j, s - j, s - j):
            copy.wait_recv()

    loop(1, n - s, st_start)
    ring(two, cut[1], cut[2])

    key_total = kv.shape[0] * kv.shape[1] * kv.shape[2]
    owners = max(1, min(n, KEY_BLOCK // (nt * rows)))
    blocks = n // owners
    scale = 1.0 / math.sqrt(QK_DIM)

    def attend(h, b):
        both = kv[:, pl.ds(b * owners, owners)].reshape(nt * owners * rows, kv.shape[3])
        values = both[:, 2 * QK_DIM :]
        parts = []
        for comp in range(2):
            lo = (2 * h + comp) * QK_DIM
            keys = both[:, comp * QK_DIM : (comp + 1) * QK_DIM]
            scores = dot(queries[:, lo : lo + QK_DIM], keys, NT) * scale
            peak = jnp.max(scores, axis=1, keepdims=True)
            expo = jnp.exp(scores - peak)
            parts += [peak, jnp.sum(expo, axis=1, keepdims=True), dot(expo.astype(BF16), values)]
        return tuple(parts)

    def merge(a, b):
        parts = []
        for comp in range(2):
            pa, ta, wa = a[3 * comp : 3 * comp + 3]
            pb, tb, wb = b[3 * comp : 3 * comp + 3]
            peak = jnp.maximum(pa, pb)
            ea, eb = jnp.exp(pa - peak), jnp.exp(pb - peak)
            parts += [peak, ta * ea + tb * eb, wa * ea + wb * eb]
        return tuple(parts)

    attn_heads = queries.shape[1] // (2 * QK_DIM)
    hidden = []
    for h in range(attn_heads):
        got = attend(h, 0)
        if blocks > 1:
            got = lax.fori_loop(1, blocks, lambda b, g: merge(g, attend(h, b)), got)
        blended = got[2] / got[1] - mapw[h] * (got[5] / got[4])
        hidden.append(rms(blended, again[...]))
        if h == 0:
            ring(two, cut[2], cut[3])
    attn_hidden = jnp.concatenate(hidden, axis=1).astype(BF16)
    ring(two, cut[3], cut[4])

    raw = project(gr).astype(F32)
    rec_query = raw * jax.nn.sigmoid(raw)
    local, lifted = [], []
    for h in range(heads):
        c = slice(h * RECURRENT_WIDTH, (h + 1) * RECURRENT_WIDTH)
        outs, lifts = [], []
        for i in range(spans):
            r = slice(i * REC_SPAN, (i + 1) * REC_SPAN)
            run = running[i][:, c]
            dq = (rec_query[r, c] * jnp.exp(run)).astype(BF16)
            within = dot(dq, (inflow[r, c] * jnp.exp(-run)).astype(BF16), NT) * lower
            o = dot(within.astype(BF16), vals[r, c])
            if befores[h][i] is not None:
                o = o + dot(dq, befores[h][i].astype(BF16), NT)
            outs.append(o)
            lifts.append(rec_query[r, c] * jnp.exp(offsets[i][:, c] + run))
        local.append(jnp.concatenate(outs, axis=0))
        lifted.append(jnp.concatenate(lifts, axis=0).astype(BF16))

    loop(1, s + 1, st_wait)
    first = tuple(init[h].T for h in range(heads))

    def chain(k, carry):
        d = jnp.exp(decay[k][0:1])
        return tuple(
            carry[h] * d[:, h * RECURRENT_WIDTH : (h + 1) * RECURRENT_WIDTH]
            + state[k, h].astype(F32)
            for h in range(heads)
        )

    incoming = lax.fori_loop(0, s, chain, first)
    rec = []
    for h in range(heads):
        o = local[h] + dot(lifted[h], incoming[h].astype(BF16), NT)
        rec.append(rms(o, rgain[...]))
    rec_hidden = jnp.concatenate(rec, axis=1).astype(BF16)

    width = nf.shape[2]
    pieces = o_send.shape[0]
    step = width // pieces

    def o_copy(i, j):
        cols = pl.ds(i * step, step)
        return pltpu.make_async_remote_copy(
            src_ref=pbuf.at[tp_peer(j), :, cols], dst_ref=rbuf.at[j, :, cols],
            send_sem=o_send.at[i, j], recv_sem=o_recv.at[i, j],
            device_id=(s, tp_peer(j)), device_id_type=MESH,
        )

    per = n // pieces
    for i in range(pieces):
        wa = goa[i * per : (i + 1) * per].reshape(step, goa.shape[2])
        wb = gor[i * per : (i + 1) * per].reshape(step, gor.shape[2])
        part = (dot(attn_hidden, wa, NT) + dot(rec_hidden, wb, NT)).astype(BF16)
        pbuf[:, :, i * step : (i + 1) * step] = part.reshape(nt, rows, step)
        for j in range(1, nt):
            o_copy(i, j).start()
    for i in range(pieces):
        cols = slice(i * step, (i + 1) * step)
        acc = pbuf[t, :, cols].astype(F32)
        for j in range(1, nt):
            o_copy(i, j).wait_recv()
            acc = acc + rbuf[j, :, cols].astype(F32)
        out[:, cols] = acc.astype(out.dtype)

    finish(one)
    finish(two)
    for j in range(1, nt):
        n_copy(j).wait_send()
        kt_copy(j).wait_send()
        for i in range(pieces):
            o_copy(i, j).wait_send()
    loop(1, n, lambda j: kv_copy(j).wait_send())

    def st_done(j):
        for copy in st_pair(j, s + j, s):
            copy.wait_send()

    loop(1, n - s, st_done)


def solution(mesh):
    n, nt = mesh.shape["sp"], mesh.shape["tp"]

    def body(
        tokens, input_norm_gain, paired_query_weight, shared_key_weight, shared_value_weight,
        recurrent_query_weight, forget_gate_weight, recurrent_value_weight,
        attention_output_weight, recurrent_output_weight, attention_head_gain,
        recurrent_head_gain, second_map_weight, forget_leak_rate, extra_log_decay,
        initial_recurrent_state,
    ):
        rows, width = tokens.shape
        heads = initial_recurrent_state.shape[0]
        weights = (
            paired_query_weight, forget_gate_weight, recurrent_value_weight,
            recurrent_query_weight, attention_output_weight, recurrent_output_weight,
        )
        half = n // 2
        pieces = 4
        vm = pl.BlockSpec(memory_space=pltpu.VMEM)
        sm = pl.BlockSpec(memory_space=pltpu.SMEM)
        dma = pltpu.SemaphoreType.DMA
        w = RECURRENT_WIDTH
        return pl.pallas_call(
            functools.partial(kernel, n, nt),
            out_shape=jax.ShapeDtypeStruct((rows, width), BF16),
            in_specs=[vm] * 12 + [sm] + [vm] * 3,
            out_specs=vm,
            scratch_shapes=[pltpu.VMEM((n,) + a.shape, BF16) for a in weights]
            + [
                pltpu.VMEM((nt, rows, width), BF16),
                pltpu.VMEM((nt, n, rows, 2 * QK_DIM + HEAD_DIM), BF16),
                pltpu.VMEM((n, heads, w, w), BF16),
                pltpu.VMEM((n, 8, heads * w), F32),
                pltpu.VMEM((nt, rows, width), BF16),
                pltpu.VMEM((nt, rows, width), BF16),
                dma((6, 2, half)), dma((6, 2, half)),
                dma((nt,)), dma((nt,)),
                dma((n,)), dma((n,)),
                dma((nt,)), dma((nt,)),
                dma((n,)), dma((n,)),
                dma((n,)), dma((n,)),
                dma((pieces, nt)), dma((pieces, nt)),
            ],
            compiler_params=pltpu.CompilerParams(
                has_side_effects=True, vmem_limit_bytes=60 * 1024 * 1024
            ),
        )(
            tokens, input_norm_gain[None], *weights, shared_key_weight, shared_value_weight,
            attention_head_gain[None], recurrent_head_gain[None], second_map_weight,
            forget_leak_rate[None], extra_log_decay, initial_recurrent_state,
        )

    placed = (
        P(("sp", "tp"), None), P(), P("sp", "tp"), P(), P(), P("sp", "tp"), P("sp", "tp"),
        P("sp", "tp"), P("sp", "tp"), P("sp", "tp"), P(), P(), P("tp"), P("tp"),
        P("sp", "tp"), P("tp", None, None),
    )
    return jax.shard_map(
        body, mesh=mesh, in_specs=placed, out_specs=P(("sp", "tp"), None), check_vma=False
    )
```

time: 255 us -> 93.6 us (0.37)
  the two profiles are of different devices: /device:TPU:0 before, /device:TPU:9 now
where the time goes in v1:
time: 93.6 us; the launch traced here: 93.4 us
  Pallas kernels  88.8 us (95%)
  local copies, waits for them, and re-layouts  4.63 us (5%)
    pallas_call x1, Pallas kernels, body(): pl.pallas_call(functools.partial(kernel, n, nt), out_shape=jax.ShapeDtype...  88.8 us
    unnamed x5, local copies, waits for them, and re-layouts  4.63 us

profile of v1, /device:TPU:9, one launch (start us, length us, event | category | flops | bytes accessed | tf_op | source)
XLA Modules:
  0.0 93.4 jit_solution(9146623829143581746)
XLA Ops:
  0.0 0.0 copy-start
  0.0 2.0 %copy.17.wk = bf16[2048,64]{1,0:T(8,128)(2,1)} copy(bf16[2048,64]{0,1:T(8,128)(2,1)} %param.19) | data formatting | bytes 524288 | tf_op args[3]
  2.0 0.0 copy-done
  2.0 1.0 %copy.18.wval = bf16[2048,64]{1,0:T(8,128)(2,1)} copy(bf16[2048,64]{0,1:T(8,128)(2,1)S(1)} %copy-done) | data formatting | bytes 524288 | tf_op args[4]
  3.0 88.8 %shard_map.154 = bf16[48,2048]{1,0:T(8,128)(2,1)} custom-call(bf16[48,2048]{1,0:T(8,128)(2,1)} %tok.1, f32[1,2048]{1,0:T(1,128)} %bitcast.4, bf16[256,128]{1,0:T(8,128)(2,1)} %wq.1, bf16[256,256]{1,0:T(8,128)(2,1)} %wg.1, bf16[256,256]{1,0:T(8,128)(2,1)} %wv.1, bf16[256,256]{1,0:T(8,128)(2,1)} %wr.1, bf16[256,128]{1,0:T(8,128)(2,1)} %woa.1, ...), custom_call_target="tpu_custom_call" | custom-call | tf_op jit(solution)/shard_map/pallas_call | solution.py:400
  91.8 1.6 %copy.20 = bf16[48,2048]{1,0:T(8,128)(2,1)} copy(bf16[48,2048]{1,0:T(8,128)(2,1)} %shard_map.154) | data formatting | bytes 393216
Async XLA Ops:
  0.0 2.0 %copy-start = (bf16[2048,64]{0,1:T(8,128)(2,1)S(1)}, bf16[2048,64]{0,1:T(8,128)(2,1)}, u32[]{:S(2)}) copy-start(bf16[2048,64]{0,1:T(8,128)(2,1)} %param.20) | copy-start | bytes 786436

commit v2 on v1

--- a/solution.py
+++ b/solution.py
@@ -42,9 +42,9 @@
     n, nt,
     tok, gain, wq, wg, wv, wr, woa, wor, wk, wval, again, rgain, mapw, leak, extra, init,
     out,
-    gq, gg, gv, gr, goa, gor, nf, kv, state, decay, pbuf, rbuf,
+    gq, gg, gv, gr, goa, gor, nf, kv, pair, pair_d, units, units_d, prefix, pbuf, rbuf,
     ring_send, ring_recv, n_send, n_recv, kv_send, kv_recv, kt_send, kt_recv,
-    st_send, st_recv, de_send, de_recv, o_send, o_recv,
+    p_send, p_recv, st_send, st_recv, de_send, de_recv, o_send, o_recv,
 ):
     s, t = lax.axis_index("sp"), lax.axis_index("tp")
     half = n // 2
@@ -58,7 +58,7 @@
 
     ins = (wq, wg, wv, wr, woa, wor)
     bufs = (gq, gg, gv, gr, goa, gor)
-    longer = (0, 0, 1, 0, 1, 1)
+    longer = (1, 0, 1, 0, 1, 1)
 
     def hops(a, d):
         return half if longer[a] == d else half - 1
@@ -115,8 +115,17 @@
                 send(a, d, 0, True).wait_send()
                 loop(1, hops(a, d), lambda k: send(a, d, k, False).wait_send())
 
-    one, two = (0, 1, 2), (3, 4, 5)
+    one, two, three = (1, 2), (3, 0), (4, 5)
     cut = [half * i // 4 for i in range(5)]
+    barrier = pltpu.get_barrier_semaphore()
+
+    def greet(peer):
+        pl.semaphore_signal(barrier, inc=1, device_id=peer, device_id_type=MESH)
+
+    loop(1, n, lambda j: greet(((s + j) % n, t)))
+    for j in range(1, nt):
+        greet((s, (t + j) % nt))
+    pl.semaphore_wait(barrier, n + nt - 2)
     start(one)
 
     rows = tok.shape[0]
@@ -140,7 +149,7 @@
         )
 
     kv[t, s] = jnp.concatenate(
-        [dot(normed, wk[...]).astype(BF16), dot(normed, wval[...]).astype(BF16)], axis=1
+        [dot(normed, wk[...], NT).astype(BF16), dot(normed, wval[...], NT).astype(BF16)], axis=1
     )
     for j in range(1, nt):
         n_copy(j).start()
@@ -193,7 +202,6 @@
     def project(buf):
         return dot(full, buf[...].reshape(full.shape[1], buf.shape[2])).astype(BF16)
 
-    queries = project(gq)
     gate = project(gg).astype(F32)
     vals = project(gv)
     ring(two, cut[0], cut[1])
@@ -213,10 +221,11 @@
         offsets.append(offset)
         offset = offset + run[REC_SPAN - 1 : REC_SPAN]
     total = offset
-    heads = log_decay.shape[1] // RECURRENT_WIDTH
+    w = RECURRENT_WIDTH
+    heads = log_decay.shape[1] // w
     befores = [[None] * spans for _ in range(heads)]
     for h in range(heads):
-        c = slice(h * RECURRENT_WIDTH, (h + 1) * RECURRENT_WIDTH)
+        c = slice(h * w, (h + 1) * w)
         carried = None
         for i in range(spans):
             r = slice(i * REC_SPAN, (i + 1) * REC_SPAN)
@@ -225,33 +234,54 @@
             weight = (inflow[r, c] * jnp.exp(final - running[i][:, c])).astype(BF16)
             new = dot(vals[r, c], weight, TN)
             carried = new if carried is None else carried * jnp.exp(final) + new
-        state[s, h] = carried.astype(BF16)
-    decay[s] = jnp.broadcast_to(total, decay.shape[1:])
+        pair[x, h] = carried.astype(BF16)
+        pair_d[x, h] = jnp.broadcast_to(total[:, c], pair_d.shape[2:])
+
+    mate = s + 1 - 2 * x
+
+    def mate_copy(i, ref):
+        return pltpu.make_async_remote_copy(
+            src_ref=ref, dst_ref=ref, send_sem=p_send.at[i], recv_sem=p_recv.at[i],
+            device_id=(mate, t), device_id_type=MESH,
+        )
 
     def st_pair(j, peer, owner):
         return (
             pltpu.make_async_remote_copy(
-                src_ref=state.at[owner], dst_ref=state.at[owner],
+                src_ref=units.at[owner], dst_ref=units.at[owner],
                 send_sem=st_send.at[j], recv_sem=st_recv.at[j],
-                device_id=(peer, t), device_id_type=MESH,
+                device_id=(2 * peer + x, t), device_id_type=MESH,
             ),
             pltpu.make_async_remote_copy(
-                src_ref=decay.at[owner], dst_ref=decay.at[owner],
+                src_ref=units_d.at[owner], dst_ref=units_d.at[owner],
                 send_sem=de_send.at[j], recv_sem=de_recv.at[j],
-                device_id=(peer, t), device_id_type=MESH,
+                device_id=(2 * peer + x, t), device_id_type=MESH,
             ),
         )
 
     def st_start(j):
-        for copy in st_pair(j, s + j, s):
+        for copy in st_pair(j, z + j, z):
             copy.start()
 
     def st_wait(j):
-        for copy in st_pair(j, s - j, s - j):
+        for copy in st_pair(j, z - j, z - j):
             copy.wait_recv()
 
-    loop(1, n - s, st_start)
+    mate_copy(0, pair.at[x]).start()
+    mate_copy(1, pair_d.at[x]).start()
     ring(two, cut[1], cut[2])
+    mate_copy(0, pair.at[1 - x]).wait_recv()
+    mate_copy(1, pair_d.at[1 - x]).wait_recv()
+    units[z] = (
+        pair[0, x].astype(F32) * jnp.exp(pair_d[1, x][0:1]) + pair[1, x].astype(F32)
+    ).astype(BF16)
+    units_d[z] = pair_d[0, x] + pair_d[1, x]
+    loop(1, half - z, st_start)
+    ring(two, cut[2], half - 1)
+    start(three)
+    ring(two, half - 1, half)
+    queries = project(gq)
+    raw = project(gr).astype(F32)
 
     key_total = kv.shape[0] * kv.shape[1] * kv.shape[2]
     owners = max(1, min(n, KEY_BLOCK // (nt * rows)))
@@ -290,11 +320,17 @@
         blended = got[2] / got[1] - mapw[h] * (got[5] / got[4])
         hidden.append(rms(blended, again[...]))
         if h == 0:
-            ring(two, cut[2], cut[3])
+            ring(three, cut[0], cut[1])
+            loop(1, z + 1, st_wait)
+
+            def chain(k, carry):
+                return carry * jnp.exp(units_d[k][0:1]) + units[k].astype(F32)
+
+            prefix[x] = lax.fori_loop(0, z, chain, init[x].T).astype(BF16)
+            mate_copy(2, prefix.at[x]).start()
     attn_hidden = jnp.concatenate(hidden, axis=1).astype(BF16)
-    ring(two, cut[3], cut[4])
-
-    raw = project(gr).astype(F32)
+    ring(three, cut[1], cut[2])
+
     rec_query = raw * jax.nn.sigmoid(raw)
     local, lifted = [], []
     for h in range(heads):
@@ -313,66 +349,80 @@
         local.append(jnp.concatenate(outs, axis=0))
         lifted.append(jnp.concatenate(lifts, axis=0).astype(BF16))
 
-    loop(1, s + 1, st_wait)
-    first = tuple(init[h].T for h in range(heads))
-
-    def chain(k, carry):
-        d = jnp.exp(decay[k][0:1])
-        return tuple(
-            carry[h] * d[:, h * RECURRENT_WIDTH : (h + 1) * RECURRENT_WIDTH]
-            + state[k, h].astype(F32)
-            for h in range(heads)
-        )
-
-    incoming = lax.fori_loop(0, s, chain, first)
+    mate_copy(2, prefix.at[1 - x]).wait_recv()
     rec = []
     for h in range(heads):
-        o = local[h] + dot(lifted[h], incoming[h].astype(BF16), NT)
+        base = prefix[h].astype(F32)
+        later = base * jnp.exp(pair_d[0, h][0:1]) + pair[0, h].astype(F32)
+        incoming = jnp.where(x == 1, later, base)
+        o = local[h] + dot(lifted[h], incoming.astype(BF16), NT)
         rec.append(rms(o, rgain[...]))
     rec_hidden = jnp.concatenate(rec, axis=1).astype(BF16)
 
-    width = nf.shape[2]
-    pieces = o_send.shape[0]
-    step = width // pieces
-
-    def o_copy(i, j):
-        cols = pl.ds(i * step, step)
-        return pltpu.make_async_remote_copy(
-            src_ref=pbuf.at[tp_peer(j), :, cols], dst_ref=rbuf.at[j, :, cols],
-            send_sem=o_send.at[i, j], recv_sem=o_recv.at[i, j],
+    part_width = pbuf.shape[3]
+
+    def o_copy(b, j):
+        return pltpu.make_async_remote_copy(
+            src_ref=pbuf.at[b, tp_peer(j)], dst_ref=rbuf.at[b, j],
+            send_sem=o_send.at[b, j], recv_sem=o_recv.at[b, j],
             device_id=(s, tp_peer(j)), device_id_type=MESH,
         )
 
-    per = n // pieces
-    for i in range(pieces):
-        wa = goa[i * per : (i + 1) * per].reshape(step, goa.shape[2])
-        wb = gor[i * per : (i + 1) * per].reshape(step, gor.shape[2])
-        part = (dot(attn_hidden, wa, NT) + dot(rec_hidden, wb, NT)).astype(BF16)
-        pbuf[:, :, i * step : (i + 1) * step] = part.reshape(nt, rows, step)
+    def out_block(b):
+        part = dot(attn_hidden, goa[b], NT) + dot(rec_hidden, gor[b], NT)
+        pbuf[b] = part.astype(BF16).reshape(nt, rows, part_width)
         for j in range(1, nt):
-            o_copy(i, j).start()
-    for i in range(pieces):
-        cols = slice(i * step, (i + 1) * step)
-        acc = pbuf[t, :, cols].astype(F32)
+            o_copy(b, j).start()
+
+    def both_sides(k):
+        out_block(at(pos - k - 1))
+        out_block(at(pos + k + 1))
+
+    def repeat(lo, hi, body):
+        if n <= 8:
+            for k in range(lo, hi):
+                body(k)
+        else:
+            loop(lo, hi, body)
+
+    def arrive(k):
+        ring_hop(three, k)
+        both_sides(k)
+
+    out_block(s)
+    repeat(0, cut[2], both_sides)
+    repeat(cut[2], half - 1, arrive)
+    ring_hop(three, half - 1)
+    out_block(at(pos + half))
+    for b in range(n):
+        acc = pbuf[b, t].astype(F32)
         for j in range(1, nt):
-            o_copy(i, j).wait_recv()
-            acc = acc + rbuf[j, :, cols].astype(F32)
-        out[:, cols] = acc.astype(out.dtype)
+            o_copy(b, j).wait_recv()
+            acc = acc + rbuf[b, j].astype(F32)
+        out[:, b * part_width : (b + 1) * part_width] = acc.astype(out.dtype)
 
     finish(one)
     finish(two)
+    finish(three)
     for j in range(1, nt):
         n_copy(j).wait_send()
         kt_copy(j).wait_send()
-        for i in range(pieces):
-            o_copy(i, j).wait_send()
     loop(1, n, lambda j: kv_copy(j).wait_send())
 
     def st_done(j):
-        for copy in st_pair(j, s + j, s):
+        for copy in st_pair(j, z + j, z):
             copy.wait_send()
 
-    loop(1, n - s, st_done)
+    loop(1, half - z, st_done)
+    mate_copy(0, pair.at[x]).wait_send()
+    mate_copy(1, pair_d.at[x]).wait_send()
+    mate_copy(2, prefix.at[x]).wait_send()
+
+    def o_done(b):
+        for j in range(1, nt):
+            o_copy(b, j).wait_send()
+
+    loop(0, n, o_done)
 
 
 def solution(mesh):
@@ -392,7 +442,6 @@
             recurrent_query_weight, attention_output_weight, recurrent_output_weight,
         )
         half = n // 2
-        pieces = 4
         vm = pl.BlockSpec(memory_space=pltpu.VMEM)
         sm = pl.BlockSpec(memory_space=pltpu.SMEM)
         dma = pltpu.SemaphoreType.DMA
@@ -406,23 +455,27 @@
             + [
                 pltpu.VMEM((nt, rows, width), BF16),
                 pltpu.VMEM((nt, n, rows, 2 * QK_DIM + HEAD_DIM), BF16),
-                pltpu.VMEM((n, heads, w, w), BF16),
-                pltpu.VMEM((n, 8, heads * w), F32),
-                pltpu.VMEM((nt, rows, width), BF16),
-                pltpu.VMEM((nt, rows, width), BF16),
+                pltpu.VMEM((2, heads, w, w), BF16),
+                pltpu.VMEM((2, heads, 8, w), F32),
+                pltpu.VMEM((half, w, w), BF16),
+                pltpu.VMEM((half, 8, w), F32),
+                pltpu.VMEM((2, w, w), BF16),
+                pltpu.VMEM((n, nt, rows, width // n), BF16),
+                pltpu.VMEM((n, nt, rows, width // n), BF16),
                 dma((6, 2, half)), dma((6, 2, half)),
                 dma((nt,)), dma((nt,)),
                 dma((n,)), dma((n,)),
                 dma((nt,)), dma((nt,)),
-                dma((n,)), dma((n,)),
-                dma((n,)), dma((n,)),
-                dma((pieces, nt)), dma((pieces, nt)),
+                dma((3,)), dma((3,)),
+                dma((half,)), dma((half,)),
+                dma((half,)), dma((half,)),
+                dma((n, nt)), dma((n, nt)),
             ],
             compiler_params=pltpu.CompilerParams(
-                has_side_effects=True, vmem_limit_bytes=60 * 1024 * 1024
+                has_side_effects=True, collective_id=0, vmem_limit_bytes=60 * 1024 * 1024
             ),
         )(
-            tokens, input_norm_gain[None], *weights, shared_key_weight, shared_value_weight,
+            tokens, input_norm_gain[None], *weights, shared_key_weight.T, shared_value_weight.T,
             attention_head_gain[None], recurrent_head_gain[None], second_map_weight,
             forget_leak_rate[None], extra_log_decay, initial_recurrent_state,
         )

time: 93.6 us -> 76.6 us (0.82)
  the two profiles are of different devices: /device:TPU:9 before, /device:TPU:0 now
where the time goes in v2:
time: 76.6 us; the launch traced here: 76.4 us
  Pallas kernels  74.8 us (98%)
  local copies, waits for them, and re-layouts  1.62 us (2%)
    pallas_call x1, Pallas kernels, body(): pl.pallas_call(functools.partial(kernel, n, nt), out_shape=jax.ShapeDtype...  74.8 us
    unnamed x1, local copies, waits for them, and re-layouts  1.62 us

profile of v2, /device:TPU:0, one launch (start us, length us, event | category | flops | bytes accessed | tf_op | source)
XLA Modules:
  0.0 76.4 jit_solution(16036140480749514381)
XLA Ops:
  0.0 74.8 %shard_map.154 = bf16[48,2048]{1,0:T(8,128)(2,1)} custom-call(bf16[48,2048]{1,0:T(8,128)(2,1)} %tok.1, f32[1,2048]{1,0:T(1,128)} %bitcast.8, bf16[256,128]{1,0:T(8,128)(2,1)} %wq.1, bf16[256,256]{1,0:T(8,128)(2,1)} %wg.1, bf16[256,256]{1,0:T(8,128)(2,1)} %wv.1, bf16[256,256]{1,0:T(8,128)(2,1)} %wr.1, bf16[256,128]{1,0:T(8,128)(2,1)} %woa.1, ...), custom_call_target="tpu_custom_call" | custom-call | tf_op jit(solution)/shard_map/pallas_call | solution.py:449
  74.8 1.6 %copy.18 = bf16[48,2048]{1,0:T(8,128)(2,1)} copy(bf16[48,2048]{1,0:T(8,128)(2,1)} %shard_map.154) | data formatting | bytes 393216

commit v3 on v2

--- a/solution.py
+++ b/solution.py
@@ -58,7 +58,7 @@
 
     ins = (wq, wg, wv, wr, woa, wor)
     bufs = (gq, gg, gv, gr, goa, gor)
-    longer = (1, 0, 1, 0, 1, 1)
+    longer = (1, 0, 1, 0, 0, 1)
 
     def hops(a, d):
         return half if longer[a] == d else half - 1

time: 76.6 us -> 76.9 us (level)
  no operation moved by 1% of the time
where the time goes in v3:
time: 76.9 us; the launch traced here: 76.7 us
  Pallas kernels  75.1 us (98%)
  local copies, waits for them, and re-layouts  1.62 us (2%)
    pallas_call x1, Pallas kernels, body(): pl.pallas_call(functools.partial(kernel, n, nt), out_shape=jax.ShapeDtype...  75.1 us
    unnamed x1, local copies, waits for them, and re-layouts  1.62 us

profile of v3, /device:TPU:0, one launch (start us, length us, event | category | flops | bytes accessed | tf_op | source)
XLA Modules:
  0.0 76.7 jit_solution(2636182960301256385)
XLA Ops:
  0.0 75.1 %shard_map.154 = bf16[48,2048]{1,0:T(8,128)(2,1)} custom-call(bf16[48,2048]{1,0:T(8,128)(2,1)} %tok.1, f32[1,2048]{1,0:T(1,128)} %bitcast.8, bf16[256,128]{1,0:T(8,128)(2,1)} %wq.1, bf16[256,256]{1,0:T(8,128)(2,1)} %wg.1, bf16[256,256]{1,0:T(8,128)(2,1)} %wv.1, bf16[256,256]{1,0:T(8,128)(2,1)} %wr.1, bf16[256,128]{1,0:T(8,128)(2,1)} %woa.1, ...), custom_call_target="tpu_custom_call" | custom-call | tf_op jit(solution)/shard_map/pallas_call | solution.py:449
  75.1 1.6 %copy.18 = bf16[48,2048]{1,0:T(8,128)(2,1)} copy(bf16[48,2048]{1,0:T(8,128)(2,1)} %shard_map.154) | data formatting | bytes 393216
